TPU v7x, 512 devices: a 4x2x32 block of a 4x8x32 slice. The times are simulated.
512 devices in a mesh: grp: 2 (over y), sp: 32 (over z), tp: 8 (over x, core).
Axes of the slice: x: 4, y: 2, z: 32, core: 2. Of those that a mesh axis runs over, the one named last changes fastest.
The devices are a block of a 4x8x32 slice.
Arguments:
- tokens: bfloat16 [32768, 2048], P(('grp', 'sp')), parts along dimension 0, may hold values from -6 to 6
- fresh_token_input: bfloat16 [4096], P('grp'), parts along dimension 0, may hold values from -6 to 6
- value_matrix: bfloat16 [2048, 2048], P(None, 'tp'), may hold values from -0.125 to 0.125
- write_matrix: bfloat16 [2048, 1024], P(None, 'tp'), may hold values from -0.125 to 0.125
- read_matrix: bfloat16 [2048, 1024], P(None, 'tp'), may hold values from -0.125 to 0.125
- gate_matrix: bfloat16 [2048, 2048], P(None, 'tp'), may hold values from -0.125 to 0.125
- step_matrix: bfloat16 [2048, 32], replicated, may hold values from -0.125 to 0.125
- value_filter_taps: bfloat16 [4, 2048], replicated, may hold values from -3 to 3
- write_filter_taps: bfloat16 [4, 1024], replicated, may hold values from -3 to 3
- read_filter_taps: bfloat16 [4, 1024], replicated, may hold values from -3 to 3
- head_log_decay: float32 [32], replicated
- step_offset_bias: float32 [32], replicated, may hold values from -3.5 to -2.5
- decay_spike: float32 [32768, 32], P(('grp', 'sp'), 'tp'), parts along dimension 0, may hold values from -3 to 0, as said below
- bypass_scale: float32 [32], replicated, may hold values from 0.5 to 2
- group_norm_scale: float32 [2048], replicated, may hold values from 0.1 to 1.9
Outputs:
- prompt_out: bfloat16 [32768, 2048], P(('grp', 'sp'), 'tp'), parts along dimension 0
- state_cache: bfloat16 [256, 2048], P(('grp', 'sp'), 'tp'), parts along dimension 0
- step_out: bfloat16 [128, 32], P(('grp', 'tp'), 'sp'), parts along dimension 0
There are 2 independent parts, one for each index of `grp`. A program takes and returns all parts, laid end to end along the dimension named above; an argument that names none is the same for every part. Nothing has to cross between parts.
Inputs may be any that keep to these rules, and one draw needn't show every extreme that they name: `decay_spike`: never positive.
All inputs are finite; a program needn't handle non-finite values.
Results may differ from a plain program's by a relative error of at most 0.023.
Values may be sent and summed in bfloat16 or wider, within the bound.
No kernel may reach another device: no remote copies, remote signals or barrier semaphores. Data moves between devices by JAX's collectives and lax.ppermute only.
A program may use at most 64 MiB of HBM per device.

v0:
```python
import jax
import jax.numpy as jnp
from jax import lax
from jax.sharding import PartitionSpec as P

HEAD = 64
STATE = 128
CONV = 4
BLOCK = 128
epsilon = 1e-06


def passed_along(block, axis, distance):
    devices = range(lax.axis_size(axis))
    route = [(i - distance, i) for i in devices if i - distance in devices]
    return lax.ppermute(block, axis, route)


def from_root(value, axis, source):
    kept = jnp.where(lax.axis_index(axis) == source, value, 0).astype(value.dtype)
    return lax.psum(kept, axis)


def in_order(pieces, dim):
    dims = list(pieces.shape[1:])
    dims[dim] *= pieces.shape[0]
    return jnp.moveaxis(pieces, 0, dim).reshape(dims)


def from_everyone(value, axis):
    peers = lax.axis_size(axis)
    return lax.all_to_all(
        jnp.broadcast_to(value[None], (peers, *value.shape)), axis, 0, 0, tiled=True
    )


def gather_directly(value, axis, dim):
    return in_order(from_everyone(value, axis), dim)


def taken_together(value, axis):
    everything = from_everyone(value, axis)
    return jnp.sum(everything, axis=0)


def project(operand, weights):
    return jnp.dot(operand, weights, preferred_element_type=jnp.float32).astype(jnp.bfloat16)


def apply_taps(previous, current, tap_weights):
    joined = jnp.concatenate([previous, current], axis=0).astype(jnp.float32)
    length = current.shape[0]
    summed = jnp.zeros(current.shape, jnp.float32)
    for offset in range(CONV):
        summed = summed + tap_weights[offset].astype(jnp.float32) * joined[offset : offset + length]
    return summed


def group_norm(gated_rows, groups):
    shaped = gated_rows.reshape(gated_rows.shape[:-1] + (groups, -1))
    normed = shaped * lax.rsqrt(jnp.mean(shaped * shaped, axis=-1, keepdims=True) + epsilon)
    return normed.reshape(gated_rows.shape)


def read_new(cached, stored_portion, read_part, new_decay, step_now, value_now):
    states = cached.astype(jnp.float32).reshape((cached.shape[0],) + value_now.shape)
    updated = (
        new_decay[None, :, :, None] * states
        + step_now[None, :, :, None] * stored_portion.T[:, :, None, None] * value_now[None]
    )
    return jnp.einsum("gn,ngep->gep", read_part, updated)


def on_device(
    tokens,
    fresh_token_input,
    value_matrix,
    write_matrix,
    read_matrix,
    gate_matrix,
    step_matrix,
    value_filter_taps,
    write_filter_taps,
    read_filter_taps,
    head_log_decay,
    step_offset_bias,
    decay_spike,
    bypass_scale,
    group_norm_scale,
):
    head_rank = lax.axis_index("tp")
    sequence_rank = lax.axis_index("sp")
    sequence_count = lax.axis_size("sp")
    channels = value_matrix.shape[1]
    head_count = channels // HEAD
    map_width = write_matrix.shape[1]
    group_count = map_width // STATE
    per_group = head_count // group_count
    row_count = tokens.shape[0]
    head_start = head_rank * head_count
    local_count = STATE // sequence_count
    own_step = lax.dynamic_slice_in_dim(step_matrix, head_start, head_count, 1)
    own_value_taps = lax.dynamic_slice_in_dim(value_filter_taps, head_rank * channels, channels, 1)
    own_write_taps = lax.dynamic_slice_in_dim(
        write_filter_taps, head_rank * map_width, map_width, 1
    )
    own_read_taps = lax.dynamic_slice_in_dim(read_filter_taps, head_rank * map_width, map_width, 1)
    head_decay_rates = jnp.exp(lax.dynamic_slice_in_dim(head_log_decay, head_start, head_count, 0))
    own_bias = lax.dynamic_slice_in_dim(step_offset_bias, head_start, head_count, 0)
    own_skip = lax.dynamic_slice_in_dim(bypass_scale, head_start, head_count, 0)
    own_gain = lax.dynamic_slice_in_dim(group_norm_scale, head_rank * channels, channels, 0)
    value_rows = project(tokens, value_matrix)
    write_rows = project(tokens, write_matrix)
    read_rows = project(tokens, read_matrix)
    gate_rows = project(tokens, gate_matrix)
    step_raw = jnp.dot(tokens, own_step, preferred_element_type=jnp.float32)
    edge = row_count - (CONV - 1)
    tail_rows = (value_rows[edge:], write_rows[edge:], read_rows[edge:])
    before = passed_along((tail_rows[0], tail_rows[1], tail_rows[2]), "sp", 1)
    ending = (
        from_root(tail_rows[0], "sp", sequence_count - 1),
        from_root(tail_rows[1], "sp", sequence_count - 1),
        from_root(tail_rows[2], "sp", sequence_count - 1),
    )
    values = jax.nn.silu(apply_taps(before[0], value_rows, own_value_taps)).astype(jnp.bfloat16)
    writes = jax.nn.silu(apply_taps(before[1], write_rows, own_write_taps)).astype(jnp.bfloat16)
    reads = jax.nn.silu(apply_taps(before[2], read_rows, own_read_taps)).astype(jnp.bfloat16)
    step_length = jax.nn.softplus(step_raw + own_bias)
    log_decay_value = decay_spike - step_length * head_decay_rates
    blocks = row_count // BLOCK
    block_values = values.reshape(blocks, BLOCK, group_count, per_group, HEAD)
    block_writes = writes.reshape(blocks, BLOCK, group_count, STATE)
    block_reads = reads.reshape(blocks, BLOCK, group_count, STATE)
    block_steps = step_length.reshape(blocks, BLOCK, group_count, per_group)
    cumulative = jnp.cumsum(log_decay_value.reshape(blocks, BLOCK, group_count, per_group), axis=1)
    block_end = cumulative[:, -1]
    scaled = (
        (jnp.exp(block_end[:, None] - cumulative) * block_steps)[..., None]
        * block_values.astype(jnp.float32)
    ).astype(jnp.bfloat16)
    block_states = jnp.einsum(
        "bsgn,bsgep->bngep", block_writes, scaled, preferred_element_type=jnp.float32
    )
    running = jnp.zeros((STATE, group_count, per_group, HEAD), jnp.float32)
    inside = []
    for block_index in range(blocks):
        inside.append(running)
        running = (
            jnp.exp(block_end[block_index])[None, :, :, None] * running + block_states[block_index]
        )
    local_states = jnp.stack(inside)
    shard_fading_factor = jnp.sum(block_end, axis=0)
    before_block = jnp.cumsum(block_end, axis=0) - block_end
    decay_table = gather_directly(shard_fading_factor[None], "sp", 0)
    inclusive = jnp.cumsum(decay_table, axis=0)
    exclusive = inclusive - decay_table
    total_decay = inclusive[-1]
    row_pieces = lax.all_to_all(running[None], "sp", split_axis=1, concat_axis=0, tiled=True)
    ranks = jnp.arange(sequence_count)
    below = (ranks[None, :] < ranks[:, None])[:, :, None, None]
    prefix_weight = jnp.exp(jnp.where(below, exclusive[:, None] - inclusive[None, :], -jnp.inf))
    prefix_rows = jnp.einsum("jkge,kngep->jngep", prefix_weight, row_pieces)
    final_weight = jnp.exp(total_decay[None] - inclusive)
    final_rows = jnp.einsum("kge,kngep->ngep", final_weight, row_pieces)
    earlier_state = lax.all_to_all(prefix_rows, "sp", split_axis=0, concat_axis=1, tiled=True)[0]
    scores = jnp.einsum(
        "blgn,bsgn->bgls", block_reads, block_writes, preferred_element_type=jnp.float32
    )
    cum_heads = jnp.transpose(cumulative, (0, 2, 3, 1))
    decay_gaps = cum_heads[..., :, None] - cum_heads[..., None, :]
    step_heads = jnp.transpose(block_steps, (0, 2, 3, 1))
    causal = jnp.tril(jnp.ones((BLOCK, BLOCK), bool))
    mixing = (
        scores[:, :, None]
        * jnp.exp(jnp.where(causal, decay_gaps, -jnp.inf))
        * step_heads[..., None, :]
    ).astype(jnp.bfloat16)
    inner_part = jnp.einsum(
        "bgels,bsgep->blgep", mixing, block_values, preferred_element_type=jnp.float32
    )
    entering = jnp.exp(before_block)[:, None, :, :, None] * earlier_state[None] + local_states
    carried_part = jnp.exp(cumulative)[..., None] * jnp.einsum(
        "blgn,bngep->blgep", block_reads.astype(jnp.float32), entering
    )
    mixed_rows = (inner_part + carried_part).reshape(row_count, head_count, HEAD) + own_skip[
        None, :, None
    ] * values.astype(jnp.float32).reshape(row_count, head_count, HEAD)
    gated_rows = mixed_rows.reshape(row_count, channels) * jax.nn.silu(
        gate_rows.astype(jnp.float32)
    )
    prompt_out = (group_norm(gated_rows, group_count) * own_gain).astype(jnp.bfloat16)
    new_row = fresh_token_input[None]
    new_value = project(new_row, value_matrix)
    new_write = project(new_row, write_matrix)
    new_read = project(new_row, read_matrix)
    new_gate = project(new_row, gate_matrix)
    new_step = jax.nn.softplus(
        jnp.dot(new_row, own_step, preferred_element_type=jnp.float32)[0] + own_bias
    )
    new_values = jax.nn.silu(apply_taps(ending[0], new_value, own_value_taps)).astype(jnp.bfloat16)
    latest_stores = jax.nn.silu(apply_taps(ending[1], new_write, own_write_taps)).astype(
        jnp.bfloat16
    )
    new_reads = jax.nn.silu(apply_taps(ending[2], new_read, own_read_taps)).astype(jnp.bfloat16)
    value_now = new_values.astype(jnp.float32).reshape(group_count, per_group, HEAD)
    write_now = latest_stores.astype(jnp.float32)
    read_now = new_reads.astype(jnp.float32)
    new_decay = jnp.exp(-new_step * head_decay_rates).reshape(group_count, per_group)
    step_now = new_step.reshape(group_count, per_group)
    row_start = sequence_rank * local_count
    cache_rows = final_rows.reshape(local_count, channels).astype(jnp.bfloat16)
    stored_portion = lax.dynamic_slice_in_dim(write_now, row_start, local_count, 1)
    read_part = lax.dynamic_slice_in_dim(read_now, row_start, local_count, 1)
    partial_value = read_new(cache_rows, stored_portion, read_part, new_decay, step_now, value_now)
    reading = taken_together(partial_value, "sp")
    new_mixed = reading + own_skip.reshape(group_count, per_group)[:, :, None] * value_now
    new_gated = new_mixed.reshape(1, channels) * jax.nn.silu(new_gate.astype(jnp.float32))
    step_whole = (group_norm(new_gated, group_count) * own_gain).astype(jnp.bfloat16)[0]
    step_table = step_whole.reshape(channels // sequence_count, sequence_count)
    step_out = lax.dynamic_slice_in_dim(step_table, sequence_rank, 1, 1)
    return (prompt_out, cache_rows, step_out)


def solution(mesh):
    placed = (
        P(("grp", "sp"), None),
        P("grp"),
        P(None, "tp"),
        P(None, "tp"),
        P(None, "tp"),
        P(None, "tp"),
        P(),
        P(),
        P(),
        P(),
        P(),
        P(),
        P(("grp", "sp"), "tp"),
        P(),
        P(),
    )
    return jax.shard_map(
        on_device,
        mesh=mesh,
        in_specs=placed,
        out_specs=(P(("grp", "sp"), "tp"), P(("grp", "sp"), "tp"), P(("grp", "tp"), "sp")),
        check_vma=False,
    )
```

profile of v0, /device:TPU:46, one launch (start us, length us, event | category | flops | bytes accessed | tf_op | source)
XLA Modules:
  0.0 264.0 jit_solution(4816721934194735863)
XLA Ops:
  0.7 1.6 copy-done
  2.2 1.8 convolution_convert_fusion.2
  4.6 5.3 %collective-permute-start.2 = (bf16[3,128]{1,0:T(4,128)(2,1)}, bf16[3,128]{1,0:T(4,128)(2,1)}, u32[]{:S(2)}, u32[]{:S(2)}) collective-permute-start(bf16[3,128]{1,0:T(4,128)(2,1)} %get-tuple-element.46), channel_id=1, source_target_pairs={{0,8},{8,16},{16,24},{24,32},{32,40},{40,48},{48,56},{56,64},{64,7... | collective-permute-start | bytes 2312 | tf_op jit(solution)/shard_map/ppermute | solution.py:16
  11.3 4.7 %collective-permute-start.1 = (bf16[3,128]{1,0:T(4,128)(2,1)}, bf16[3,128]{1,0:T(4,128)(2,1)}, u32[]{:S(2)}, u32[]{:S(2)}) collective-permute-start(bf16[3,128]{1,0:T(4,128)(2,1)} %get-tuple-element.44), channel_id=1, source_target_pairs={{0,8},{8,16},{16,24},{24,32},{32,40},{40,48},{48,56},{56,64},{64,7... | collective-permute-start | bytes 2312 | tf_op jit(solution)/shard_map/ppermute | solution.py:16
  16.1 1.5 multiply_exponential_fusion
  17.5 1.4 multiply_subtract_fusion
  20.6 43.0 %all-to-all-start.1 = ((f32[32,1,1,4]{3,2,1,0:T(1,128)}), f32[32,1,1,4]{3,2,1,0:T(1,128)}, u32[]{:S(2)}, u32[]{:S(2)}) async-start(f32[32,1,1,4]{3,2,1,0:T(1,128)} %broadcast_in_dim.36), calls=%async_computation.1 | async-start | bytes 32768 | tf_op jit(solution)/shard_map/all_to_all | solution.py:32
  63.6 1.9 convolution_convert_fusion.1
  66.8 3.8 %collective-permute-start = (bf16[3,256]{1,0:T(4,128)(2,1)}, bf16[3,256]{1,0:T(4,128)(2,1)}, u32[]{:S(2)}, u32[]{:S(2)}) collective-permute-start(bf16[3,256]{1,0:T(4,128)(2,1)} %get-tuple-element.42), channel_id=1, source_target_pairs={{0,8},{8,16},{16,24},{24,32},{32,40},{40,48},{48,56},{56,64},{64,7... | collective-permute-start | bytes 4616 | tf_op jit(solution)/shard_map/ppermute | solution.py:16
  72.2 1.5 fusion.89
  76.5 2.1 fusion.90
  79.9 56.4 %all-reduce = (bf16[3,256]{1,0:T(4,128)(2,1)S(1)}, bf16[3,128]{1,0:T(4,128)(2,1)S(1)}, bf16[3,128]{1,0:T(4,128)(2,1)S(1)}) all-reduce(bf16[3,256]{1,0:T(4,128)(2,1)S(1)} %copy-done.13, bf16[3,128]{1,0:T(4,128)(2,1)S(1)} %copy-done.18, bf16[3,128]{1,0:T(4,128)(2,1)S(1)} %copy-done.19), channel_id=1, replica_groups=mesh['grp'=2,'sp'=32,'tp'=8] {'sp'}, use_global_device_ids=true, to_apply=%region_7.8 | all-reduce | flops 1536 | bytes 6144 | tf_op jit(solution)/shard_map/psum | solution.py:21
  137.6 2.2 fusion.85
  149.1 19.8 %all-to-all-start = ((bf16[32,2,512]{2,1,0:T(2,128)(2,1)}), bf16[32,2,512]{2,1,0:T(2,128)(2,1)S(1)}, u32[]{:S(2)}, u32[]{:S(2)}) async-start(bf16[32,2,512]{2,1,0:T(2,128)(2,1)} %reshape.495), calls=%async_computation | async-start | bytes 131072 | tf_op jit(solution)/shard_map/all_to_all | solution.py:158
  170.7 22.1 %all-to-all-done = bf16[32,2,512]{2,1,0:T(2,128)(2,1)S(1)} async-done(((bf16[32,2,512]{2,1,0:T(2,128)(2,1)}), bf16[32,2,512]{2,1,0:T(2,128)(2,1)S(1)}, u32[]{:S(2)}, u32[]{:S(2)}) %all-to-all-start) | async-done | bytes 65568 | tf_op jit(solution)/shard_map/all_to_all | solution.py:158
  194.1 5.3 %all-to-all-start.3 = ((f32[32,1,256]{2,1,0:T(1,128)}), f32[32,1,256]{2,1,0:T(1,128)}, u32[]{:S(2)}, u32[]{:S(2)}) async-start(f32[32,1,256]{2,1,0:T(1,128)} %reshape.499), calls=%async_computation.3 | async-start | bytes 65536 | tf_op jit(solution)/shard_map/all_to_all | solution.py:32
  200.8 21.1 %all-to-all-done.3 = f32[32,1,256]{2,1,0:T(1,128)} async-done(((f32[32,1,256]{2,1,0:T(1,128)}), f32[32,1,256]{2,1,0:T(1,128)}, u32[]{:S(2)}, u32[]{:S(2)}) %all-to-all-start.3) | async-done | bytes 32800 | tf_op jit(solution)/shard_map/all_to_all | solution.py:32
  221.8 5.0 %all-to-all-start.2 = ((f32[32,1,1024]{2,1,0:T(1,128)}), f32[32,1,1024]{2,1,0:T(1,128)S(1)}, u32[]{:S(2)}, u32[]{:S(2)}) async-start(f32[32,1,1024]{2,1,0:T(1,128)} %reshape.497), calls=%async_computation.2 | async-start | bytes 262144 | tf_op jit(solution)/shard_map/all_to_all | solution.py:165
  228.1 1.6 fusion.52
  230.9 1.5 reduce.19
  236.7 16.4 %all-to-all-done.2 = f32[32,1,1024]{2,1,0:T(1,128)S(1)} async-done(((f32[32,1,1024]{2,1,0:T(1,128)}), f32[32,1,1024]{2,1,0:T(1,128)S(1)}, u32[]{:S(2)}, u32[]{:S(2)}) %all-to-all-start.2) | async-done | bytes 131104 | tf_op jit(solution)/shard_map/all_to_all | solution.py:165
  255.9 2.1 fusion
  258.0 1.4 copy.186
  260.9 2.2 multiply_reduce_fusion
  (153 shorter events, 36.4 us)
Async XLA Ops:
  0.6 9.3 %copy-start.2 = (bf16[2048,128]{1,0:T(8,128)(2,1)S(1)}, bf16[2048,128]{1,0:T(8,128)(2,1)}, u32[]{:S(2)}) copy-start(bf16[2048,128]{1,0:T(8,128)(2,1)} %param.19) | copy-start | bytes 1572868
  2.2 13.7 %copy-start.17 = (bf16[2048]{0:T(1024)(128)(2,1)S(1)}, bf16[2048]{0:T(1024)(128)(2,1)}, u32[]{:S(2)}) copy-start(bf16[2048]{0:T(1024)(128)(2,1)} %param.16) | copy-start | bytes 12292
  2.2 13.7 %copy-start.27 = (f32[32]{0:T(128)S(1)}, f32[32]{0:T(128)}, u32[]{:S(2)}) copy-start(f32[32]{0:T(128)} %param.26) | copy-start | bytes 388
  2.2 13.8 %copy-start.28 = (f32[32]{0:T(128)S(1)}, f32[32]{0:T(128)}, u32[]{:S(2)}) copy-start(f32[32]{0:T(128)} %param.25) | copy-start | bytes 388
  4.0 13.5 %copy-start.12 = (f32[512,4]{0,1:T(4,128)S(1)}, f32[512,4]{0,1:T(4,128)}, u32[]{:S(2)}) copy-start(f32[512,4]{0,1:T(4,128)} %param.27) | copy-start | bytes 24580
  4.6 139.3 %collective-permute-start.2 = (bf16[3,128]{1,0:T(4,128)(2,1)}, bf16[3,128]{1,0:T(4,128)(2,1)}, u32[]{:S(2)}, u32[]{:S(2)}) collective-permute-start(bf16[3,128]{1,0:T(4,128)(2,1)} %get-tuple-element.46), channel_id=1, source_target_pairs={{0,8},{8,16},{16,24},{24,32},{32,40},{40,48},{48,56},{56,64},{64,7... | collective-permute-start | bytes 2312 | tf_op jit(solution)/shard_map/ppermute | solution.py:16
  10.6 8.4 %copy-start.3 = (bf16[512,128]{1,0:T(8,128)(2,1)}, bf16[512,128]{1,0:T(8,128)(2,1)S(1)}, u32[]{:S(2)}) copy-start(bf16[512,128]{1,0:T(8,128)(2,1)S(1)} %convolution_convert_fusion.3) | copy-start | bytes 393220
  11.3 131.8 %collective-permute-start.1 = (bf16[3,128]{1,0:T(4,128)(2,1)}, bf16[3,128]{1,0:T(4,128)(2,1)}, u32[]{:S(2)}, u32[]{:S(2)}) collective-permute-start(bf16[3,128]{1,0:T(4,128)(2,1)} %get-tuple-element.44), channel_id=1, source_target_pairs={{0,8},{8,16},{16,24},{24,32},{32,40},{40,48},{48,56},{56,64},{64,7... | collective-permute-start | bytes 2312 | tf_op jit(solution)/shard_map/ppermute | solution.py:16
  19.3 51.9 %copy-start.1 = (bf16[2048,128]{1,0:T(8,128)(2,1)S(1)}, bf16[2048,128]{1,0:T(8,128)(2,1)}, u32[]{:S(2)}) copy-start(bf16[2048,128]{1,0:T(8,128)(2,1)} %param.18) | copy-start | bytes 1572868
  20.6 128.6 %all-to-all-start.1 = ((f32[32,1,1,4]{3,2,1,0:T(1,128)}), f32[32,1,1,4]{3,2,1,0:T(1,128)}, u32[]{:S(2)}, u32[]{:S(2)}) async-start(f32[32,1,1,4]{3,2,1,0:T(1,128)} %broadcast_in_dim.36), calls=%async_computation.1 | async-start | bytes 32768 | tf_op jit(solution)/shard_map/all_to_all | solution.py:32
  66.8 78.9 %collective-permute-start = (bf16[3,256]{1,0:T(4,128)(2,1)}, bf16[3,256]{1,0:T(4,128)(2,1)}, u32[]{:S(2)}, u32[]{:S(2)}) collective-permute-start(bf16[3,256]{1,0:T(4,128)(2,1)} %get-tuple-element.42), channel_id=1, source_target_pairs={{0,8},{8,16},{16,24},{24,32},{32,40},{40,48},{48,56},{56,64},{64,7... | collective-permute-start | bytes 4616 | tf_op jit(solution)/shard_map/ppermute | solution.py:16
  72.0 7.9 %copy-start.19 = (bf16[3,128]{1,0:T(4,128)(2,1)S(1)}, bf16[3,128]{1,0:T(4,128)(2,1)}, u32[]{:S(2)}) copy-start(bf16[3,128]{1,0:T(4,128)(2,1)} %get-tuple-element.43) | copy-start | bytes 2308
  72.0 64.3 %copy-start.20 = (bf16[1,128]{1,0:T(2,128)(2,1)S(1)}, bf16[1,128]{1,0:T(2,128)(2,1)}, u32[]{:S(2)}) copy-start(bf16[1,128]{1,0:T(2,128)(2,1)} %fusion.5) | copy-start | bytes 772
  72.0 65.0 %copy-start.26 = (f32[4]{0:T(128)S(1)}, f32[4]{0:T(128)}, u32[]{:S(2)}) copy-start(f32[4]{0:T(128)} %get-tuple-element.57) | copy-start | bytes 52
  72.0 71.1 %copy-start.4 = (bf16[512,128]{1,0:T(8,128)(2,1)S(1)}, bf16[512,128]{1,0:T(8,128)(2,1)}, u32[]{:S(2)}) copy-start(bf16[512,128]{1,0:T(8,128)(2,1)} %copy-done.3) | copy-start | bytes 393220
  78.6 67.2 %copy-start.7 = (bf16[512,256]{1,0:T(8,128)(2,1)S(1)}, bf16[512,256]{1,0:T(8,128)(2,1)}, u32[]{:S(2)}) copy-start(bf16[512,256]{1,0:T(8,128)(2,1)} %copy-done.6) | copy-start | bytes 786436
  146.9 46.2 %copy-start.24 = (f32[4]{0:T(128)S(1)}, f32[4]{0:T(128)}, u32[]{:S(2)}) copy-start(f32[4]{0:T(128)} %get-tuple-element.25) | copy-start | bytes 52
  146.9 46.3 %copy-start.25 = (bf16[1,128]{1,0:T(2,128)(2,1)S(1)}, bf16[1,128]{1,0:T(2,128)(2,1)}, u32[]{:S(2)}) copy-start(bf16[1,128]{1,0:T(2,128)(2,1)} %fusion.80) | copy-start | bytes 772
  147.0 52.4 %copy-start.10 = (pred[32,32]{1,0:T(8,128)(4,1)S(1)}, pred[32,32]{1,0:T(8,128)(4,1)}, u32[]{:S(2)}) copy-start(pred[32,32]{1,0:T(8,128)(4,1)} %iota_compare_fusion.1) | copy-start | bytes 3076
  149.1 43.7 %all-to-all-start = ((bf16[32,2,512]{2,1,0:T(2,128)(2,1)}), bf16[32,2,512]{2,1,0:T(2,128)(2,1)S(1)}, u32[]{:S(2)}, u32[]{:S(2)}) async-start(bf16[32,2,512]{2,1,0:T(2,128)(2,1)} %reshape.495), calls=%async_computation | async-start | bytes 131072 | tf_op jit(solution)/shard_map/all_to_all | solution.py:158
  194.1 27.7 %all-to-all-start.3 = ((f32[32,1,256]{2,1,0:T(1,128)}), f32[32,1,256]{2,1,0:T(1,128)}, u32[]{:S(2)}, u32[]{:S(2)}) async-start(f32[32,1,256]{2,1,0:T(1,128)} %reshape.499), calls=%async_computation.3 | async-start | bytes 65536 | tf_op jit(solution)/shard_map/all_to_all | solution.py:32
  200.8 55.1 %copy-start.8 = (f32[4,128,128]{2,1,0:T(8,128)S(1)}, f32[4,128,128]{2,1,0:T(8,128)}, u32[]{:S(2)}) copy-start(f32[4,128,128]{2,1,0:T(8,128)} %fusion.88) | copy-start | bytes 786436
  221.8 31.3 %all-to-all-start.2 = ((f32[32,1,1024]{2,1,0:T(1,128)}), f32[32,1,1024]{2,1,0:T(1,128)S(1)}, u32[]{:S(2)}, u32[]{:S(2)}) async-start(f32[32,1,1024]{2,1,0:T(1,128)} %reshape.497), calls=%async_computation.2 | async-start | bytes 262144 | tf_op jit(solution)/shard_map/all_to_all | solution.py:165
  229.8 26.1 %copy-start.11 = (pred[128,128]{1,0:T(8,128)(4,1)S(1)}, pred[128,128]{1,0:T(8,128)(4,1)}, u32[]{:S(2)}) copy-start(pred[128,128]{1,0:T(8,128)(4,1)} %iota_compare_fusion) | copy-start | bytes 49156
  (12 other events, 36.7 us)
where the time goes:
time: 265 us; the launch traced here: 264 us
  starting transfers between devices  86.9 us (33%)
  waiting for transfers between devices  59.6 us (22%)
  blocking collectives  56.4 us (21%)
  other arithmetic  21.9 us (8%)
  matrix products  19.2 us (7%)
  local copies, waits for them, and re-layouts  18 us (7%)
    psum x1, blocking collectives, from_root(): return lax.psum(kept, axis)  56.4 us
    all_to_all x2, starting transfers between devices, from_everyone(): lax.all_to_all(jnp.broadcast_to(value[None], (peers, *value.shape)), axis...  48.4 us
    all_to_all x1, waiting for transfers between devices, on_device(): lax.all_to_all(running[None], 'sp', split_axis=1, concat_axis=0, tiled=True)  22.1 us
    all_to_all x2, waiting for transfers between devices, from_everyone(): lax.all_to_all(jnp.broadcast_to(value[None], (peers, *value.shape)), axis...  21.1 us
    all_to_all x1, starting transfers between devices, on_device(): lax.all_to_all(running[None], 'sp', split_axis=1, concat_axis=0, tiled=True)  19.8 us
    all_to_all x1, waiting for transfers between devices, on_device(): lax.all_to_all(prefix_rows, 'sp', split_axis=0, concat_axis=1, tiled=True)  16.4 us
    ppermute x3, starting transfers between devices, passed_along(): return lax.ppermute(block, axis, route)  13.8 us
    dot_general x8, matrix products, project(): jnp.dot(operand, weights, preferred_element_type=jnp.float32)  11.1 us
  transfers between devices with their start and end apart: 7, of which 3 were waited for; matrix products, arithmetic and copies ran while one was open for 16% of the time, Pallas kernels for 0%

commit v1 on v0

--- a/solution.py
+++ b/solution.py
@@ -18,7 +18,7 @@
 
 def from_root(value, axis, source):
     kept = jnp.where(lax.axis_index(axis) == source, value, 0).astype(value.dtype)
-    return lax.psum(kept, axis)
+    return jnp.sum(lax.all_gather(kept, axis), axis=0)
 
 
 def in_order(pieces, dim):

time: 265 us -> 370 us (1.40)
  blocking collectives: 56.4 us -> 161 us
    all_gather x0 -> x3, blocking collectives: none -> 161 us  [from_root(): return jnp.sum(lax.all_gather(kept, axis), axis=0)]
    psum x1 -> x0, blocking collectives: 56.4 us -> none  [from_root(): return lax.psum(kept, axis)]
  transfers between devices with their start and end apart: 7 -> 7, of which waited for: 3 -> 3; matrix products, arithmetic and copies ran while one was open for 16% -> 12% of each run, Pallas kernels for 0% -> 0%
where the time goes in v1:
time: 370 us; the launch traced here: 369 us
  blocking collectives  161 us (44%)
  starting transfers between devices  86 us (23%)
  waiting for transfers between devices  59.8 us (16%)
  other arithmetic  22 us (6%)
  matrix products  19.1 us (5%)
  local copies, waits for them, and re-layouts  18.7 us (5%)
    all_gather x3, blocking collectives, from_root(): return jnp.sum(lax.all_gather(kept, axis), axis=0)  161 us
    all_to_all x2, starting transfers between devices, from_everyone(): lax.all_to_all(jnp.broadcast_to(value[None], (peers, *value.shape)), axis...  48.4 us
    all_to_all x1, waiting for transfers between devices, on_device(): lax.all_to_all(running[None], 'sp', split_axis=1, concat_axis=0, tiled=True)  22.1 us
    all_to_all x2, waiting for transfers between devices, from_everyone(): lax.all_to_all(jnp.broadcast_to(value[None], (peers, *value.shape)), axis...  21.1 us
    all_to_all x1, starting transfers between devices, on_device(): lax.all_to_all(running[None], 'sp', split_axis=1, concat_axis=0, tiled=True)  18.9 us
    all_to_all x1, waiting for transfers between devices, on_device(): lax.all_to_all(prefix_rows, 'sp', split_axis=0, concat_axis=1, tiled=True)  16.6 us
    ppermute x3, starting transfers between devices, passed_along(): return lax.ppermute(block, axis, route)  13.8 us
    dot_general x8, matrix products, project(): jnp.dot(operand, weights, preferred_element_type=jnp.float32)  11.1 us
  transfers between devices with their start and end apart: 7, of which 3 were waited for; matrix products, arithmetic and copies ran while one was open for 12% of the time, Pallas kernels for 0%

profile of v1, /device:TPU:46, one launch (start us, length us, event | category | flops | bytes accessed | tf_op | source)
XLA Modules:
  0.0 368.7 jit_solution(13538097520180829)
XLA Ops:
  0.7 1.6 copy-done
  2.2 1.8 convolution_convert_fusion.2
  4.6 5.2 %collective-permute-start.2 = (bf16[3,128]{1,0:T(4,128)(2,1)}, bf16[3,128]{1,0:T(4,128)(2,1)}, u32[]{:S(2)}, u32[]{:S(2)}) collective-permute-start(bf16[3,128]{1,0:T(4,128)(2,1)} %get-tuple-element.43), channel_id=1, source_target_pairs={{0,8},{8,16},{16,24},{24,32},{32,40},{40,48},{48,56},{56,64},{64,7... | collective-permute-start | bytes 2312 | tf_op jit(solution)/shard_map/ppermute | solution.py:16
  11.2 4.7 %collective-permute-start.1 = (bf16[3,128]{1,0:T(4,128)(2,1)}, bf16[3,128]{1,0:T(4,128)(2,1)}, u32[]{:S(2)}, u32[]{:S(2)}) collective-permute-start(bf16[3,128]{1,0:T(4,128)(2,1)} %get-tuple-element.41), channel_id=1, source_target_pairs={{0,8},{8,16},{16,24},{24,32},{32,40},{40,48},{48,56},{56,64},{64,7... | collective-permute-start | bytes 2312 | tf_op jit(solution)/shard_map/ppermute | solution.py:16
  20.5 43.0 %all-to-all-start.1 = ((f32[32,1,1,4]{3,2,1,0:T(1,128)}), f32[32,1,1,4]{3,2,1,0:T(1,128)}, u32[]{:S(2)}, u32[]{:S(2)}) async-start(f32[32,1,1,4]{3,2,1,0:T(1,128)} %broadcast_in_dim.36), calls=%async_computation.1 | async-start | bytes 32768 | tf_op jit(solution)/shard_map/all_to_all | solution.py:32
  63.5 1.9 convolution_convert_fusion.1
  66.7 3.8 %collective-permute-start = (bf16[3,256]{1,0:T(4,128)(2,1)}, bf16[3,256]{1,0:T(4,128)(2,1)}, u32[]{:S(2)}, u32[]{:S(2)}) collective-permute-start(bf16[3,256]{1,0:T(4,128)(2,1)} %get-tuple-element.39), channel_id=1, source_target_pairs={{0,8},{8,16},{16,24},{24,32},{32,40},{40,48},{48,56},{56,64},{64,7... | collective-permute-start | bytes 4616 | tf_op jit(solution)/shard_map/ppermute | solution.py:16
  72.1 1.5 fusion.89
  77.1 2.0 fusion.90
  79.2 54.9 %all-gather.4 = bf16[32,3,128]{2,1,0:T(4,128)(2,1)S(1)} all-gather(bf16[1,3,128]{2,1,0:T(4,128)(2,1)S(1)} %copy-done.19), channel_id=3, replica_groups=mesh['grp'=2,'sp'=32,'tp'=8] {'sp'}, dimensions={0}, use_global_device_ids=true | all-gather | bytes 25344 | tf_op jit(solution)/shard_map/all_gather | solution.py:21
  134.2 52.2 %all-gather.3 = bf16[32,3,128]{2,1,0:T(4,128)(2,1)S(1)} all-gather(bf16[1,3,128]{2,1,0:T(4,128)(2,1)S(1)} %copy-done.18), channel_id=2, replica_groups=mesh['grp'=2,'sp'=32,'tp'=8] {'sp'}, dimensions={0}, use_global_device_ids=true | all-gather | bytes 25344 | tf_op jit(solution)/shard_map/all_gather | solution.py:21
  188.2 54.1 %all-gather.5 = bf16[32,3,256]{2,1,0:T(4,128)(2,1)S(1)} all-gather(bf16[1,3,256]{2,1,0:T(4,128)(2,1)S(1)} %copy-done.13), channel_id=4, replica_groups=mesh['grp'=2,'sp'=32,'tp'=8] {'sp'}, dimensions={0}, use_global_device_ids=true | all-gather | bytes 50688 | tf_op jit(solution)/shard_map/all_gather | solution.py:21
  243.1 2.2 fusion.85
  254.6 18.9 %all-to-all-start = ((bf16[32,2,512]{2,1,0:T(2,128)(2,1)}), bf16[32,2,512]{2,1,0:T(2,128)(2,1)S(1)}, u32[]{:S(2)}, u32[]{:S(2)}) async-start(bf16[32,2,512]{2,1,0:T(2,128)(2,1)} %reshape.507), calls=%async_computation | async-start | bytes 131072 | tf_op jit(solution)/shard_map/all_to_all | solution.py:158
  275.2 22.1 %all-to-all-done = bf16[32,2,512]{2,1,0:T(2,128)(2,1)S(1)} async-done(((bf16[32,2,512]{2,1,0:T(2,128)(2,1)}), bf16[32,2,512]{2,1,0:T(2,128)(2,1)S(1)}, u32[]{:S(2)}, u32[]{:S(2)}) %all-to-all-start) | async-done | bytes 65568 | tf_op jit(solution)/shard_map/all_to_all | solution.py:158
  298.6 5.3 %all-to-all-start.3 = ((f32[32,1,256]{2,1,0:T(1,128)}), f32[32,1,256]{2,1,0:T(1,128)}, u32[]{:S(2)}, u32[]{:S(2)}) async-start(f32[32,1,256]{2,1,0:T(1,128)} %reshape.511), calls=%async_computation.3 | async-start | bytes 65536 | tf_op jit(solution)/shard_map/all_to_all | solution.py:32
  305.3 21.1 %all-to-all-done.3 = f32[32,1,256]{2,1,0:T(1,128)} async-done(((f32[32,1,256]{2,1,0:T(1,128)}), f32[32,1,256]{2,1,0:T(1,128)}, u32[]{:S(2)}, u32[]{:S(2)}) %all-to-all-start.3) | async-done | bytes 32800 | tf_op jit(solution)/shard_map/all_to_all | solution.py:32
  326.4 5.0 %all-to-all-start.2 = ((f32[32,1,1024]{2,1,0:T(1,128)}), f32[32,1,1024]{2,1,0:T(1,128)S(1)}, u32[]{:S(2)}, u32[]{:S(2)}) async-start(f32[32,1,1024]{2,1,0:T(1,128)} %reshape.509), calls=%async_computation.2 | async-start | bytes 262144 | tf_op jit(solution)/shard_map/all_to_all | solution.py:165
  332.7 1.6 fusion.52
  335.6 1.5 reduce.25
  341.3 16.6 %all-to-all-done.2 = f32[32,1,1024]{2,1,0:T(1,128)S(1)} async-done(((f32[32,1,1024]{2,1,0:T(1,128)}), f32[32,1,1024]{2,1,0:T(1,128)S(1)}, u32[]{:S(2)}, u32[]{:S(2)}) %all-to-all-start.2) | async-done | bytes 131104 | tf_op jit(solution)/shard_map/all_to_all | solution.py:165
  360.6 2.1 fusion
  362.7 1.4 copy.186
  365.6 2.2 multiply_reduce_fusion
  (159 shorter events, 40.0 us)
Async XLA Ops:
  2.2 13.7 %copy-start.17 = (bf16[2048]{0:T(1024)(128)(2,1)S(1)}, bf16[2048]{0:T(1024)(128)(2,1)}, u32[]{:S(2)}) copy-start(bf16[2048]{0:T(1024)(128)(2,1)} %param.16) | copy-start | bytes 12292
  2.2 13.7 %copy-start.27 = (f32[32]{0:T(128)S(1)}, f32[32]{0:T(128)}, u32[]{:S(2)}) copy-start(f32[32]{0:T(128)} %param.26) | copy-start | bytes 388
  2.2 13.8 %copy-start.28 = (f32[32]{0:T(128)S(1)}, f32[32]{0:T(128)}, u32[]{:S(2)}) copy-start(f32[32]{0:T(128)} %param.25) | copy-start | bytes 388
  4.0 13.5 %copy-start.12 = (f32[512,4]{0,1:T(4,128)S(1)}, f32[512,4]{0,1:T(4,128)}, u32[]{:S(2)}) copy-start(f32[512,4]{0,1:T(4,128)} %param.27) | copy-start | bytes 24580
  4.6 244.8 %collective-permute-start.2 = (bf16[3,128]{1,0:T(4,128)(2,1)}, bf16[3,128]{1,0:T(4,128)(2,1)}, u32[]{:S(2)}, u32[]{:S(2)}) collective-permute-start(bf16[3,128]{1,0:T(4,128)(2,1)} %get-tuple-element.43), channel_id=1, source_target_pairs={{0,8},{8,16},{16,24},{24,32},{32,40},{40,48},{48,56},{56,64},{64,7... | collective-permute-start | bytes 2312 | tf_op jit(solution)/shard_map/ppermute | solution.py:16
  11.2 237.4 %collective-permute-start.1 = (bf16[3,128]{1,0:T(4,128)(2,1)}, bf16[3,128]{1,0:T(4,128)(2,1)}, u32[]{:S(2)}, u32[]{:S(2)}) collective-permute-start(bf16[3,128]{1,0:T(4,128)(2,1)} %get-tuple-element.41), channel_id=1, source_target_pairs={{0,8},{8,16},{16,24},{24,32},{32,40},{40,48},{48,56},{56,64},{64,7... | collective-permute-start | bytes 2312 | tf_op jit(solution)/shard_map/ppermute | solution.py:16
  19.3 51.9 %copy-start.1 = (bf16[2048,128]{1,0:T(8,128)(2,1)S(1)}, bf16[2048,128]{1,0:T(8,128)(2,1)}, u32[]{:S(2)}) copy-start(bf16[2048,128]{1,0:T(8,128)(2,1)} %param.18) | copy-start | bytes 1572868
  20.5 234.2 %all-to-all-start.1 = ((f32[32,1,1,4]{3,2,1,0:T(1,128)}), f32[32,1,1,4]{3,2,1,0:T(1,128)}, u32[]{:S(2)}, u32[]{:S(2)}) async-start(f32[32,1,1,4]{3,2,1,0:T(1,128)} %broadcast_in_dim.36), calls=%async_computation.1 | async-start | bytes 32768 | tf_op jit(solution)/shard_map/all_to_all | solution.py:32
  66.7 184.5 %collective-permute-start = (bf16[3,256]{1,0:T(4,128)(2,1)}, bf16[3,256]{1,0:T(4,128)(2,1)}, u32[]{:S(2)}, u32[]{:S(2)}) collective-permute-start(bf16[3,256]{1,0:T(4,128)(2,1)} %get-tuple-element.39), channel_id=1, source_target_pairs={{0,8},{8,16},{16,24},{24,32},{32,40},{40,48},{48,56},{56,64},{64,7... | collective-permute-start | bytes 4616 | tf_op jit(solution)/shard_map/ppermute | solution.py:16
  71.9 62.3 %copy-start.20 = (bf16[1,128]{1,0:T(2,128)(2,1)S(1)}, bf16[1,128]{1,0:T(2,128)(2,1)}, u32[]{:S(2)}) copy-start(bf16[1,128]{1,0:T(2,128)(2,1)} %fusion.5) | copy-start | bytes 772
  71.9 62.3 %copy-start.18 = (bf16[1,3,128]{2,1,0:T(4,128)(2,1)S(1)}, bf16[1,3,128]{2,1,0:T(4,128)(2,1)}, u32[]{:S(2)}) copy-start(bf16[1,3,128]{2,1,0:T(4,128)(2,1)} %get-tuple-element.40) | copy-start | bytes 2308
  71.9 115.1 %copy-start.9 = (f32[4,1,1,4]{3,2,1,0:T(1,128)S(1)}, f32[4,1,1,4]{3,2,1,0:T(1,128)}, u32[]{:S(2)}) copy-start(f32[4,1,1,4]{3,2,1,0:T(1,128)} %get-tuple-element.33) | copy-start | bytes 196
  71.9 116.3 %copy-start.13 = (bf16[1,3,256]{2,1,0:T(4,128)(2,1)S(1)}, bf16[1,3,256]{2,1,0:T(4,128)(2,1)}, u32[]{:S(2)}) copy-start(bf16[1,3,256]{2,1,0:T(4,128)(2,1)} %get-tuple-element.38) | copy-start | bytes 4612
  71.9 170.6 %copy-start.26 = (f32[4]{0:T(128)S(1)}, f32[4]{0:T(128)}, u32[]{:S(2)}) copy-start(f32[4]{0:T(128)} %get-tuple-element.54) | copy-start | bytes 52
  71.9 176.7 %copy-start.4 = (bf16[512,128]{1,0:T(8,128)(2,1)S(1)}, bf16[512,128]{1,0:T(8,128)(2,1)}, u32[]{:S(2)}) copy-start(bf16[512,128]{1,0:T(8,128)(2,1)} %copy-done.3) | copy-start | bytes 393220
  188.2 63.0 %copy-start.7 = (bf16[512,256]{1,0:T(8,128)(2,1)S(1)}, bf16[512,256]{1,0:T(8,128)(2,1)}, u32[]{:S(2)}) copy-start(bf16[512,256]{1,0:T(8,128)(2,1)} %copy-done.6) | copy-start | bytes 786436
  252.4 45.3 %copy-start.24 = (f32[4]{0:T(128)S(1)}, f32[4]{0:T(128)}, u32[]{:S(2)}) copy-start(f32[4]{0:T(128)} %get-tuple-element.22) | copy-start | bytes 52
  252.4 45.4 %copy-start.25 = (bf16[1,128]{1,0:T(2,128)(2,1)S(1)}, bf16[1,128]{1,0:T(2,128)(2,1)}, u32[]{:S(2)}) copy-start(bf16[1,128]{1,0:T(2,128)(2,1)} %fusion.80) | copy-start | bytes 772
  252.5 51.5 %copy-start.10 = (pred[32,32]{1,0:T(8,128)(4,1)S(1)}, pred[32,32]{1,0:T(8,128)(4,1)}, u32[]{:S(2)}) copy-start(pred[32,32]{1,0:T(8,128)(4,1)} %iota_compare_fusion.1) | copy-start | bytes 3076
  254.6 42.7 %all-to-all-start = ((bf16[32,2,512]{2,1,0:T(2,128)(2,1)}), bf16[32,2,512]{2,1,0:T(2,128)(2,1)S(1)}, u32[]{:S(2)}, u32[]{:S(2)}) async-start(bf16[32,2,512]{2,1,0:T(2,128)(2,1)} %reshape.507), calls=%async_computation | async-start | bytes 131072 | tf_op jit(solution)/shard_map/all_to_all | solution.py:158
  298.6 27.8 %all-to-all-start.3 = ((f32[32,1,256]{2,1,0:T(1,128)}), f32[32,1,256]{2,1,0:T(1,128)}, u32[]{:S(2)}, u32[]{:S(2)}) async-start(f32[32,1,256]{2,1,0:T(1,128)} %reshape.511), calls=%async_computation.3 | async-start | bytes 65536 | tf_op jit(solution)/shard_map/all_to_all | solution.py:32
  305.3 55.3 %copy-start.8 = (f32[4,128,128]{2,1,0:T(8,128)S(1)}, f32[4,128,128]{2,1,0:T(8,128)}, u32[]{:S(2)}) copy-start(f32[4,128,128]{2,1,0:T(8,128)} %fusion.88) | copy-start | bytes 786436
  326.4 31.5 %all-to-all-start.2 = ((f32[32,1,1024]{2,1,0:T(1,128)}), f32[32,1,1024]{2,1,0:T(1,128)S(1)}, u32[]{:S(2)}, u32[]{:S(2)}) async-start(f32[32,1,1024]{2,1,0:T(1,128)} %reshape.509), calls=%async_computation.2 | async-start | bytes 262144 | tf_op jit(solution)/shard_map/all_to_all | solution.py:165
  334.4 26.2 %copy-start.11 = (pred[128,128]{1,0:T(8,128)(4,1)S(1)}, pred[128,128]{1,0:T(8,128)(4,1)}, u32[]{:S(2)}) copy-start(pred[128,128]{1,0:T(8,128)(4,1)} %iota_compare_fusion) | copy-start | bytes 49156
  (12 other events, 39.1 us)
